TPU v7x, 32 devices: a whole 2x2x4 slice. The times are simulated.
32 devices in a mesh: ep: 8 (over z, x), tp: 4 (over y, core).
Axes of the slice: x: 2, y: 2, z: 4, core: 2. Of those that a mesh axis runs over, the one named last changes fastest.
Arguments:
- query_latent: bfloat16 [1024, 512], P('ep'), may hold values from -6 to 6
- key_latent: bfloat16 [1024, 256], P('ep'), may hold values from -6 to 6
- rope_key: bfloat16 [1024, 64], P('ep'), may hold values from -500 to 500
- query_gain: float32 [512], replicated, may hold values from 0.1 to 1.9
- key_gain: float32 [256], replicated, may hold values from 0.1 to 1.9
- w_query: bfloat16 [512, 1024], P(None, 'tp'), may hold values from -0.25 to 0.25
- w_query_rope: bfloat16 [512, 512], P(None, 'tp'), may hold values from -0.25 to 0.25
- w_key: bfloat16 [256, 1024], P(None, 'tp'), may hold values from -0.375 to 0.375
- w_value: bfloat16 [256, 1024], P(None, 'tp'), may hold values from -0.375 to 0.375
- w_out: bfloat16 [1024, 2048], P('tp'), may hold values from -1.796875 to 1.796875
- tokens_b: bfloat16 [4096, 2048], P('ep'), may hold values from -6 to 6
- ffn_gain: float32 [2048], replicated, may hold values from 0.1 to 1.9
- route_expert: int32 [4096, 2], P('ep'), may hold values from 0 to 7, as said below
- route_weight: float32 [4096, 2], P('ep'), may hold values from 0.2 to 1
- w_gate: bfloat16 [8, 2048, 1024], P('ep', None, 'tp'), may hold values from -0.125 to 0.125
- w_up: bfloat16 [8, 2048, 1024], P('ep', None, 'tp'), may hold values from -0.125 to 0.125
- w_down: bfloat16 [8, 1024, 2048], P('ep', 'tp'), may hold values from -0.1875 to 0.1875
Outputs:
- mixer_out: bfloat16 [1024, 2048], P(('ep', 'tp'))
- moe_out: bfloat16 [4096, 2048], P('ep', 'tp')
Inputs may be any that keep to these rules, and one draw needn't show every extreme that they name: `route_expert`: expert e belongs to group e // 2. A row's 2 experts differ and lie in one group. Among the rows of one device along ep, every group is named by exactly 128 rows and every expert is named exactly 128 times.
All inputs are finite; a program needn't handle non-finite values.
Results may differ from a plain program's by a relative error of at most 0.013.
The roundings to bfloat16 on the way count: a program that leaves them out, or rounds other values in their place, can miss the bound.
Values may be sent and summed in bfloat16 or wider, within the bound.
A program may use at most 64 MiB of HBM per device.

v0:
```python
import math

import jax
import jax.numpy as jnp
from jax import lax
from jax.sharding import PartitionSpec as P

NOPE = 128
ROPE = 64
VDIM = 128
GRID_W = 64
TOPK = 2


epsilon = 1e-06
rotary_base = 10000.0
neg_large = -1e30


def rms_scale(values_in, gain):
    widened = values_in.astype(jnp.float32)
    normed = widened * lax.rsqrt(jnp.mean(widened * widened, axis=-1, keepdims=True) + epsilon)
    return (normed * gain).astype(jnp.bfloat16)


def rotary_tables(positions):
    half_width = ROPE // 2
    inverse = rotary_base ** (-jnp.arange(0, half_width, 2, dtype=jnp.float32) / half_width)
    grid_row = (positions // GRID_W).astype(jnp.float32)
    grid_col = (positions % GRID_W).astype(jnp.float32)
    angle = jnp.concatenate([grid_row[:, None] * inverse, grid_col[:, None] * inverse], axis=-1)
    return (jnp.cos(angle), jnp.sin(angle))


def rotate(values_in, cosine, sine):
    even_part = values_in[..., 0::2]
    odd_part = values_in[..., 1::2]
    turned = jnp.stack(
        [even_part * cosine - odd_part * sine, even_part * sine + odd_part * cosine], axis=-1
    )
    return turned.reshape(values_in.shape)


def fold_blocks(carry, members, step_fn):
    piece_rows = members[0].shape[0]
    block_rows = math.gcd(piece_rows, 1024)
    if block_rows == piece_rows:
        return step_fn(carry, members)
    stacked = tuple(
        (
            member.reshape((piece_rows // block_rows, block_rows) + member.shape[1:])
            for member in members
        )
    )

    def scan_step(inner_carry, blocks):
        return (step_fn(inner_carry, blocks), None)

    result, unused = lax.scan(scan_step, carry, stacked)
    return result


def mixer_half(
    query_latent,
    key_latent,
    rope_key,
    query_gain,
    key_gain,
    w_query,
    w_query_rope,
    w_key,
    w_value,
    w_out,
):
    tok_rows = query_latent.shape[0]
    local_heads = w_query.shape[1] // NOPE
    positions = lax.axis_index("ep") * tok_rows + jnp.arange(tok_rows, dtype=jnp.int32)
    cosine, sine = rotary_tables(positions)
    query_normed = rms_scale(query_latent, query_gain)
    query_nope = jnp.dot(query_normed, w_query, preferred_element_type=jnp.float32).astype(
        jnp.bfloat16
    )
    query_nope = query_nope.reshape(tok_rows, local_heads, NOPE)
    query_rot = jnp.dot(query_normed, w_query_rope, preferred_element_type=jnp.float32)
    query_rot = rotate(
        query_rot.reshape(tok_rows, local_heads, ROPE), cosine[:, None, :], sine[:, None, :]
    )
    query_rot = query_rot.astype(jnp.bfloat16)
    key_rot = rotate(rope_key.astype(jnp.float32), cosine, sine).astype(jnp.bfloat16)
    score_scale = (NOPE + ROPE) ** (-0.5)

    def expand(latent_rows):
        latent_count = latent_rows.shape[0]
        key_normed = rms_scale(latent_rows, key_gain)
        key_nope = jnp.dot(key_normed, w_key, preferred_element_type=jnp.float32).astype(
            jnp.bfloat16
        )
        value_rows = jnp.dot(key_normed, w_value, preferred_element_type=jnp.float32).astype(
            jnp.bfloat16
        )
        return (
            key_nope.reshape(latent_count, local_heads, NOPE),
            value_rows.reshape(latent_count, local_heads, VDIM),
        )

    def attend_block(carry, key_nope, value_rows, key_turn):
        run_max, run_total, run_acc = carry
        scores = jnp.einsum(
            "qhd,khd->hqk", query_nope, key_nope, preferred_element_type=jnp.float32
        )
        scores = scores + jnp.einsum(
            "qhd,kd->hqk", query_rot, key_turn, preferred_element_type=jnp.float32
        )
        scores = scores * score_scale
        new_max = jnp.maximum(run_max, jnp.max(scores, axis=-1))
        correction = jnp.exp(run_max - new_max)
        weights = jnp.exp(scores - new_max[..., None])
        new_total = run_total * correction + jnp.sum(weights, axis=-1)
        added = jnp.einsum(
            "hqk,khd->qhd",
            weights.astype(jnp.bfloat16),
            value_rows,
            preferred_element_type=jnp.float32,
        )
        new_acc = run_acc * jnp.transpose(correction)[..., None] + added
        return (new_max, new_total, new_acc)

    def step_latent(carry, blocks):
        key_nope, value_rows = expand(blocks[0])
        return attend_block(carry, key_nope, value_rows, blocks[1])

    initial = (
        jnp.full((local_heads, tok_rows), neg_large, jnp.float32),
        jnp.zeros((local_heads, tok_rows), jnp.float32),
        jnp.zeros((tok_rows, local_heads, VDIM), jnp.float32),
    )
    final = fold_blocks(
        initial,
        (
            lax.all_gather(key_latent, "ep", axis=0, tiled=True),
            lax.all_gather(key_rot, "ep", axis=0, tiled=True),
        ),
        step_latent,
    )
    run_max, run_total, run_acc = final
    heads_out = (run_acc / jnp.transpose(run_total)[..., None]).astype(jnp.bfloat16)
    heads_out = heads_out.reshape(tok_rows, local_heads * VDIM)
    return lax.psum_scatter(
        jnp.dot(heads_out, w_out, preferred_element_type=jnp.float32).astype(jnp.bfloat16),
        "tp",
        scatter_dimension=0,
        tiled=True,
    )


def expert_half(tokens_b, ffn_gain, route_expert, route_weight, w_gate, w_up, w_down):
    tok_rows = tokens_b.shape[0]
    expert_count = lax.axis_size("ep")
    capacity = TOPK * tok_rows // expert_count
    normed = rms_scale(tokens_b, ffn_gain)
    copies = route_expert.reshape(tok_rows * TOPK)
    chosen = (copies[:, None] == jnp.arange(expert_count, dtype=jnp.int32)[None, :]).astype(
        jnp.int32
    )
    earlier = jnp.cumsum(chosen, axis=0) - chosen
    slot_index = jnp.sum(earlier * chosen, axis=1)
    target = copies * capacity + slot_index
    source_row = (
        jnp.zeros((expert_count * capacity,), jnp.int32)
        .at[target]
        .set(jnp.arange(tok_rows * TOPK, dtype=jnp.int32) // TOPK)
    )
    outgoing = jnp.take(normed, source_row, axis=0)
    share_cols = outgoing.shape[1] // lax.axis_size("tp")
    own_cols = lax.dynamic_slice_in_dim(outgoing, lax.axis_index("tp") * share_cols, share_cols, 1)
    arrived = lax.all_to_all(own_cols, "ep", split_axis=0, concat_axis=0, tiled=True)
    member = lax.all_gather(arrived, "tp", axis=1, tiled=True)
    gate_rows = w_gate[0]
    up_rows = w_up[0]
    gate_act = jnp.dot(member, gate_rows, preferred_element_type=jnp.float32)
    up_act = jnp.dot(member, up_rows, preferred_element_type=jnp.float32)
    hidden = (jax.nn.silu(gate_act) * up_act).astype(jnp.bfloat16)
    partial_term = jnp.dot(hidden, w_down[0], preferred_element_type=jnp.float32)
    shared = lax.psum_scatter(
        partial_term.astype(jnp.bfloat16), "tp", scatter_dimension=1, tiled=True
    )
    returned = lax.all_to_all(shared, "ep", split_axis=0, concat_axis=0, tiled=True)
    picked = (
        jnp.take(returned, target, axis=0)
        .astype(jnp.float32)
        .reshape(tok_rows, TOPK, returned.shape[1])
    )
    combined = jnp.sum(picked * route_weight[:, :, None], axis=1)
    return combined.astype(jnp.bfloat16)


def body(
    query_latent,
    key_latent,
    rope_key,
    query_gain,
    key_gain,
    w_query,
    w_query_rope,
    w_key,
    w_value,
    w_out,
    tokens_b,
    ffn_gain,
    route_expert,
    route_weight,
    w_gate,
    w_up,
    w_down,
):
    mixer_out = mixer_half(
        query_latent,
        key_latent,
        rope_key,
        query_gain,
        key_gain,
        w_query,
        w_query_rope,
        w_key,
        w_value,
        w_out,
    )
    moe_out = expert_half(tokens_b, ffn_gain, route_expert, route_weight, w_gate, w_up, w_down)
    return (mixer_out, moe_out)


def solution(mesh):
    in_specs = (
        P("ep", None),
        P("ep", None),
        P("ep", None),
        P(),
        P(),
        P(None, "tp"),
        P(None, "tp"),
        P(None, "tp"),
        P(None, "tp"),
        P("tp", None),
        P("ep", None),
        P(),
        P("ep", None),
        P("ep", None),
        P("ep", None, "tp"),
        P("ep", None, "tp"),
        P("ep", "tp", None),
    )
    out_specs = (P(("ep", "tp"), None), P("ep", "tp"))
    return jax.shard_map(body, mesh=mesh, in_specs=in_specs, out_specs=out_specs, check_vma=False)
```

profile of v0, /device:TPU:0, one launch (start us, length us, event | category | flops | bytes accessed | tf_op | source)
XLA Modules:
  0.0 206.5 jit_solution(17284445992472675687)
XLA Ops:
  7.2 0.0 all-gather.2.cloned.1.call-start
  7.2 0.9 copy.40
  8.1 0.2 eq.28
  8.3 0.2 reshape.227
  8.5 0.7 broadcast_multiply_fusion.2
  9.2 2.3 %reduce-window.6 = s32[8,8,128]{2,1,0:T(8,128)S(1)} reduce-window(s32[8,8,128]{2,1,0:T(8,128)S(1)} %fusion.43, s32[]{:T(128)} %constant.106.clone.1), window={size=1x1x128 pad=0_0x0_0x127_0}, to_apply=%region_5.6 | reduce-window | flops 1040384 | bytes 65540 | tf_op jit(solution)/shard_map/reduce-window
  11.5 0.3 slice_reduce_fusion
  11.7 0.2 reduce-window.9
  11.9 0.1 add_bitcast_fusion
  12.0 0.2 copy.44
  12.1 0.2 mul.225
  12.4 4.3 %scatter_custom_fusion = s32[1024]{0:T(1024)S(1)} fusion(s32[1024]{0:T(1024)S(1)} %bitcast.101, s32[1024]{0:T(1024)S(1)} %add_select_fusion, s32[]{:T(128)} %constant.106.clone.1), kind=kCustom, calls=%fused_computation.95 | custom fusion | bytes 4100 | tf_op jit(solution)/shard_map/scatter | solution.py:171
  16.7 2.1 %fusion = f32[512]{0:T(512)S(1)} fusion(bf16[512,2048]{1,0:T(8,128)(2,1)} %param.27), kind=kLoop, calls=%fused_computation.5 | loop fusion | flops 3145216 | bytes 2099200 | tf_op jit(solution)/shard_map/reduce_sum | solution.py:22
  18.8 2.1 %fusion.2 = bf16[512,2048]{1,0:T(8,128)(2,1)S(1)} fusion(bf16[512,2048]{1,0:T(8,128)(2,1)} %param.27, f32[2048]{0:T(1024)} %param.28, f32[512]{0:T(512)S(1)} %add_rsqrt_fusion.1), kind=kLoop, calls=%fused_computation.7 | loop fusion | flops 4194304 | bytes 4204544 | tf_op jit(solution)/shard_map/convert_element_type | solution.py:23
  20.9 6.0 %gather_fusion = bf16[1024,2048]{1,0:T(8,128)(2,1)} fusion(bf16[512,2048]{1,0:T(8,128)(2,1)S(1)} %fusion.2, s32[1024]{0:T(1024)S(1)} %fusion.53), kind=kCustom, calls=%fused_computation | custom fusion | bytes 8392704 | tf_op jit(solution)/shard_map/jit(_take)/gather | solution.py:173
  27.0 1.6 dynamic-slice_select_fusion
  28.6 32.9 %all_to_all.24 = bf16[8,128,512]{2,1,0:T(8,128)(2,1)} all-to-all(bf16[8,128,512]{2,1,0:T(8,128)(2,1)S(1)} %bitcast.92), channel_id=1, replica_groups=mesh['ep'=8,'tp'=4] {'ep'}, dimensions={0} | all-to-all | bytes 2097152 | tf_op jit(solution)/shard_map/all_to_all | solution.py:176
  61.6 0.0 reduce-scatter.5.cloned.1.call-start
  61.6 33.6 %all-gather.2.cloned.1.call-done = bf16[1024,2048]{1,0:T(8,128)(2,1)} async-done(((bf16[1024,512]{1,0:T(8,128)(2,1)}), bf16[1024,2048]{1,0:T(8,128)(2,1)}) %all-gather.2.cloned.1.call-update) | async-done | bytes 4194320 | tf_op jit(solution)/shard_map/all_gather | solution.py:177
  95.2 4.5 %fusion.16 = f32[1024,256]{1,0:T(8,128)} fusion(bf16[1024,2048]{1,0:T(8,128)(2,1)} %all-gather.2.cloned.1.call-done, bf16[1,2048,256]{2,1,0:T(8,128)(2,1)S(1)} %copy-done.11), kind=kOutput, calls=%fused_computation.33 | convolution fusion | flops 1073741824 | bytes 6291456 | tf_op jit(solution)/shard_map/dot_general | solution.py:180
  99.8 8.8 %convolution_convert_fusion = bf16[1024,2048]{1,0:T(8,128)(2,1)} fusion(bf16[1024,2048]{1,0:T(8,128)(2,1)} %all-gather.2.cloned.1.call-done, bf16[1,256,2048]{2,1,0:T(8,128)(2,1)S(1)} %copy-done, bf16[1,2048,256]{2,1,0:T(8,128)(2,1)S(1)} %copy-done.12, f32[1024,256]{1,0:T(8,128)} %fusion.16), kind=kOutput, calls=%fused_computation.8 | convolution fusion | flops 2151153664 | bytes 11534336 | tf_op jit(solution)/shard_map/dot_general | solution.py:183
  108.6 0.6 copy-done.7
  109.3 0.2 copy-done.2
  109.5 0.1 fusion.28
  109.6 0.3 fusion.37
  110.0 0.1 broadcast_multiply_fusion.1
  110.0 0.1 fusion.48
  110.2 26.2 %all_gather.10 = bf16[1024,64]{0,1:T(8,128)(2,1)S(1)} all-gather(bf16[128,64]{0,1:T(8,128)(2,1)S(1)} %bitcast.99), channel_id=1, replica_groups=mesh['ep'=8,'tp'=4] {'ep'}, dimensions={0}, use_global_device_ids=true | all-gather | bytes 147456 | tf_op jit(solution)/shard_map/all_gather | solution.py:141
  136.4 0.2 fusion.9
  136.7 31.4 %all_gather.9 = bf16[1024,256]{1,0:T(8,128)(2,1)S(1)} all-gather(bf16[128,256]{1,0:T(8,128)(2,1)S(1)} %copy-done.6), channel_id=1, replica_groups=mesh['ep'=8,'tp'=4] {'ep'}, dimensions={0}, use_global_device_ids=true | all-gather | bytes 589824 | tf_op jit(solution)/shard_map/all_gather | solution.py:140
  168.1 0.2 fusion.10
  168.3 0.5 convolution_convert_fusion.3
  168.8 0.3 fusion.34
  169.1 0.4 fusion.59
  169.6 4.3 %all-to-all-start.1 = ((bf16[8,128,512]{2,1,0:T(8,128)(2,1)}), bf16[8,128,512]{2,1,0:T(8,128)(2,1)S(1)}, u32[]{:S(2)}, u32[]{:S(2)}) async-start(bf16[8,128,512]{2,1,0:T(8,128)(2,1)} %bitcast.93), calls=%async_computation.3 | async-start | bytes 2097152 | tf_op jit(solution)/shard_map/all_to_all | solution.py:187
  173.9 0.2 reduce-scatter.3.cloned.1.call-start
  174.2 0.3 fusion.23
  174.5 1.5 convolution_convert_fusion.2
  176.1 0.4 fusion.8
  176.5 1.2 convolution_convert_fusion.1
  177.6 0.2 reduce_sum.65
  177.8 0.1 copy.42
  178.0 0.2 copy.43
  178.2 0.1 copy.45
  178.4 12.0 %all-to-all-done.1 = bf16[8,128,512]{2,1,0:T(8,128)(2,1)S(1)} async-done(((bf16[8,128,512]{2,1,0:T(8,128)(2,1)}), bf16[8,128,512]{2,1,0:T(8,128)(2,1)S(1)}, u32[]{:S(2)}, u32[]{:S(2)}) %all-to-all-start.1) | async-done | bytes 1048608 | tf_op jit(solution)/shard_map/all_to_all | solution.py:187
  190.3 4.0 %gather_fusion.1 = bf16[1024,512]{1,0:T(8,128)(2,1)S(1)} fusion(bf16[1024,512]{1,0:T(8,128)(2,1)S(1)} %bitcast.90, s32[1024]{0:T(1024)S(1)} %broadcast_clamp_fusion), kind=kCustom, calls=%fused_computation.1 | custom fusion | bytes 2101248 | tf_op jit(solution)/shard_map/jit(_take)/gather | solution.py:189
  194.3 0.4 gather.12
  194.7 5.2 %multiply_reduce_fusion = bf16[512,512]{1,0:T(8,128)(2,1)} fusion(bf16[512,2,512]{2,1,0:T(2,128)(2,1)S(1)} %gather.12, pred[512,2]{1,0:T(8,128)(4,1)S(1)} %copy.43, f32[512,2]{1,0:T(8,128)S(1)} %copy.45), kind=kLoop, calls=%fused_computation.10 | loop fusion | flops 1835008 | bytes 1577984 | tf_op jit(solution)/shard_map/reduce_sum | solution.py:193
  (59 shorter events, 0.4 us)
Async XLA Ops:
  7.2 92.6 %copy-start = (bf16[1,256,2048]{2,1,0:T(8,128)(2,1)S(1)}, bf16[1,256,2048]{2,1,0:T(8,128)(2,1)}, u32[]{:S(2)}) copy-start(bf16[1,256,2048]{2,1,0:T(8,128)(2,1)} %param.33) | copy-start | bytes 3145732
  7.2 88.1 %all-gather.2.cloned.1.call-start = ((), (), s32[]{:S(2)}) async-start(), calls=%async_computation.5 | async-start | bytes 5242880 | tf_op jit(solution)/shard_map/all_gather | solution.py:177
  27.0 68.3 %copy-start.11 = (bf16[1,2048,256]{2,1,0:T(8,128)(2,1)S(1)}, bf16[1,2048,256]{2,1,0:T(8,128)(2,1)}, u32[]{:S(2)}) copy-start(bf16[1,2048,256]{2,1,0:T(8,128)(2,1)} %param.31) | copy-start | bytes 3145732
  61.6 38.2 %copy-start.12 = (bf16[1,2048,256]{2,1,0:T(8,128)(2,1)S(1)}, bf16[1,2048,256]{2,1,0:T(8,128)(2,1)}, u32[]{:S(2)}) copy-start(bf16[1,2048,256]{2,1,0:T(8,128)(2,1)} %param.32) | copy-start | bytes 3145732
  61.6 108.0 %reduce-scatter.5.cloned.1.call-start = ((), (), s32[]{:S(2)}) async-start(), calls=%async_computation.6 | async-start | bytes 5242880 | tf_op jit(solution)/shard_map/reduce_scatter | solution.py:184
  108.6 0.7 copy-start.7
  108.6 0.9 copy-start.2
  108.6 1.0 copy-start.5
  108.6 1.0 copy-start.9
  108.6 27.9 %copy-start.4 = (bf16[512,256]{1,0:T(8,128)(2,1)S(1)}, bf16[512,256]{1,0:T(8,128)(2,1)}, u32[]{:S(2)}) copy-start(bf16[512,256]{1,0:T(8,128)(2,1)} %param.22) | copy-start | bytes 786436
  108.6 28.1 %copy-start.6 = (bf16[128,256]{1,0:T(8,128)(2,1)S(1)}, bf16[128,256]{1,0:T(8,128)(2,1)}, u32[]{:S(2)}) copy-start(bf16[128,256]{1,0:T(8,128)(2,1)} %param.18) | copy-start | bytes 196612
  108.6 59.7 %copy-start.13 = (bf16[256,256]{1,0:T(8,128)(2,1)S(1)}, bf16[256,256]{1,0:T(8,128)(2,1)}, u32[]{:S(2)}) copy-start(bf16[256,256]{1,0:T(8,128)(2,1)} %param.24) | copy-start | bytes 393220
  108.6 59.7 %copy-start.15 = (f32[256]{0:T(256)S(1)}, f32[256]{0:T(256)}, u32[]{:S(2)}) copy-start(f32[256]{0:T(256)} %param.21) | copy-start | bytes 3076
  168.1 1.1 copy-start.1
  168.3 6.2 %copy-start.14 = (bf16[256,256]{1,0:T(8,128)(2,1)S(1)}, bf16[256,256]{1,0:T(8,128)(2,1)}, u32[]{:S(2)}) copy-start(bf16[256,256]{1,0:T(8,128)(2,1)} %param.25) | copy-start | bytes 393220
  169.6 8.4 %copy-start.8 = (s32[512,2]{0,1:T(2,128)S(1)}, s32[512,2]{0,1:T(2,128)}, u32[]{:S(2)}) copy-start(s32[512,2]{0,1:T(2,128)} %param.29) | copy-start | bytes 12292
  169.6 8.6 %copy-start.10 = (f32[512,2]{0,1:T(2,128)S(1)}, f32[512,2]{0,1:T(2,128)}, u32[]{:S(2)}) copy-start(f32[512,2]{0,1:T(2,128)} %param.30) | copy-start | bytes 12292
  169.6 20.7 %all-to-all-start.1 = ((bf16[8,128,512]{2,1,0:T(8,128)(2,1)}), bf16[8,128,512]{2,1,0:T(8,128)(2,1)S(1)}, u32[]{:S(2)}, u32[]{:S(2)}) async-start(bf16[8,128,512]{2,1,0:T(8,128)(2,1)} %bitcast.93), calls=%async_computation.3 | async-start | bytes 2097152 | tf_op jit(solution)/shard_map/all_to_all | solution.py:187
  173.9 26.0 %reduce-scatter.3.cloned.1.call-start = ((), (), s32[]{:S(2)}) async-start(), calls=%async_computation.4 | async-start | bytes 655360 | tf_op jit(solution)/shard_map/reduce_scatter | solution.py:148
  174.2 2.3 %copy-start.3 = (bf16[256,2048]{1,0:T(8,128)(2,1)S(1)}, bf16[256,2048]{1,0:T(8,128)(2,1)}, u32[]{:S(2)}) copy-start(bf16[256,2048]{1,0:T(8,128)(2,1)} %param.26) | copy-start | bytes 3145732
Sparse Core Ops, SparseCore 0:
  61.7 33.4 all-gather.1
  108.8 44.3 reduce-scatter.4
  177.8 22.1 reduce-scatter.2
where the time goes:
time: 207 us; the launch traced here: 206 us
  blocking collectives  90.5 us (44%)
  waiting for transfers between devices  45.7 us (22%)
  local copies, waits for them, and re-layouts  18.2 us (9%)
  matrix products  18.1 us (9%)
  other arithmetic  15.2 us (7%)
  between operations  14.2 us (7%)
  starting transfers between devices  4.65 us (2%)
    all_gather x1, waiting for transfers between devices, expert_half(): member = lax.all_gather(arrived, 'tp', axis=1, tiled=True)  33.6 us
    all_to_all x1, blocking collectives, expert_half(): lax.all_to_all(own_cols, 'ep', split_axis=0, concat_axis=0, tiled=True)  32.9 us
    all_gather x1, blocking collectives, mixer_half(): lax.all_gather(key_latent, 'ep', axis=0, tiled=True)  31.4 us
    all_gather x1, blocking collectives, mixer_half(): lax.all_gather(key_rot, 'ep', axis=0, tiled=True)  26.2 us
    all_to_all x1, waiting for transfers between devices, expert_half(): lax.all_to_all(shared, 'ep', split_axis=0, concat_axis=0, tiled=True)  12 us
    dot_general x1, matrix products, expert_half(): jnp.dot(hidden, w_down[0], preferred_element_type=jnp.float32)  8.8 us
    gather x1, local copies, waits for them, and re-layouts, expert_half(): outgoing = jnp.take(normed, source_row, axis=0)  6.02 us
    reduce_sum x1, other arithmetic, expert_half(): combined = jnp.sum(picked * route_weight[:, :, None], axis=1)  5.21 us
  transfers between devices with their start and end apart: 4, of which 2 were waited for; matrix products, arithmetic and copies ran while one was open for 8% of the time, Pallas kernels for 0%

commit v1 on v0

--- a/solution.py
+++ b/solution.py
@@ -3,6 +3,8 @@
 import jax
 import jax.numpy as jnp
 from jax import lax
+from jax.experimental import pallas as pl
+from jax.experimental.pallas import tpu as pltpu
 from jax.sharding import PartitionSpec as P
 
 NOPE = 128
@@ -10,6 +12,10 @@
 VDIM = 128
 GRID_W = 64
 TOPK = 2
+GROUPS = 4
+MESH = pl.DeviceIdType.MESH
+SPLIT_NUM, SPLIT_DEN = 3, 8
+JOIN_FIRST = (1, 3)
 
 
 epsilon = 1e-06
@@ -134,14 +140,11 @@
         jnp.zeros((local_heads, tok_rows), jnp.float32),
         jnp.zeros((tok_rows, local_heads, VDIM), jnp.float32),
     )
-    final = fold_blocks(
-        initial,
-        (
-            lax.all_gather(key_latent, "ep", axis=0, tiled=True),
-            lax.all_gather(key_rot, "ep", axis=0, tiled=True),
-        ),
-        step_latent,
-    )
+    gathered = lax.all_gather(
+        jnp.concatenate([key_latent, key_rot], axis=1), "ep", axis=0, tiled=True
+    )
+    rank = key_latent.shape[1]
+    final = fold_blocks(initial, (gathered[:, :rank], gathered[:, rank:]), step_latent)
     run_max, run_total, run_acc = final
     heads_out = (run_acc / jnp.transpose(run_total)[..., None]).astype(jnp.bfloat16)
     heads_out = heads_out.reshape(tok_rows, local_heads * VDIM)
@@ -192,6 +195,401 @@
     )
     combined = jnp.sum(picked * route_weight[:, :, None], axis=1)
     return combined.astype(jnp.bfloat16)
+
+
+def flip(index, distance):
+    low = index % 2
+    high = index // 2
+    if distance % 2 == 1:
+        low = 1 - low
+    if distance // 2 == 1:
+        high = 1 - high
+    return high * 2 + low
+
+
+def expert_kernel(
+    tokens_ref,
+    gain_ref,
+    order_ref,
+    weight_ref,
+    gate_hbm,
+    up_hbm,
+    down_hbm,
+    fin_ref,
+    normed_ref,
+    outgoing_ref,
+    member_ref,
+    gate_ref,
+    up_ref,
+    down_ref,
+    weight_in,
+    pair_send,
+    pair_keep,
+    pair_recv,
+    first_send,
+    first_keep,
+    first_recv,
+    second_send,
+    second_keep,
+    second_recv,
+    fin_send,
+    load_sem,
+    z_send,
+    z_recv,
+    w_send,
+    w_recv,
+    x_send,
+    x_recv,
+    y_send,
+    y_recv,
+    c_send,
+    c_recv,
+    p_send,
+    p_recv,
+    f_send,
+    f_recv,
+    s_send,
+    s_recv,
+    o_send,
+    o_recv,
+):
+    ep = lax.axis_index("ep")
+    tp = lax.axis_index("tp")
+    z, x = ep // 2, ep % 2
+    y, c = tp // 2, tp % 2
+    rows = outgoing_ref.shape[2]
+    half = outgoing_ref.shape[3]
+    tok_rows = tokens_ref.shape[0]
+    share = fin_ref.shape[2]
+    spare = rows * SPLIT_NUM // SPLIT_DEN
+    carried = pl.ds(pl.multiple_of(y * spare, 16), rows - spare)
+    passed = pl.ds(pl.multiple_of(y * (rows - spare), 16), spare)
+
+    def at_z(distance):
+        return {"ep": flip(z, distance) * 2 + x, "tp": tp}
+
+    at_x = {"ep": z * 2 + 1 - x, "tp": tp}
+    at_y = {"ep": ep, "tp": (1 - y) * 2 + c}
+    at_c = {"ep": ep, "tp": y * 2 + 1 - c}
+
+    barrier = pltpu.get_barrier_semaphore()
+    for peer in (at_z(1), at_z(2), at_z(3), at_x, at_y, at_c):
+        pl.semaphore_signal(barrier, inc=1, device_id=peer, device_id_type=MESH)
+
+    loads = [
+        pltpu.make_async_copy(gate_hbm.at[0], gate_ref, load_sem.at[0]),
+        pltpu.make_async_copy(up_hbm.at[0], up_ref, load_sem.at[1]),
+    ]
+    for t in range(4):
+        loads.append(
+            pltpu.make_async_copy(
+                down_hbm.at[0, :, pl.ds(t * share, share)], down_ref.at[t], load_sem.at[2 + t]
+            )
+        )
+    for load in loads:
+        load.start()
+
+    step_rows = 32
+
+    def norm_step(step, unused):
+        lines = pl.ds(pl.multiple_of(step * step_rows, step_rows), step_rows)
+        widened = tokens_ref[lines, :].astype(jnp.float32)
+        mean = jnp.mean(widened * widened, axis=-1, keepdims=True)
+        normed = widened * lax.rsqrt(mean + epsilon) * gain_ref[...]
+        normed_ref[lines, :] = normed.astype(jnp.bfloat16)
+        return unused
+
+    lax.fori_loop(0, tok_rows // step_rows, norm_step, 0)
+
+    def permuted(group, part):
+        lines = pl.ds(pl.multiple_of(group * rows, rows), rows)
+        return jnp.dot(
+            order_ref[lines, :],
+            normed_ref[:, part * half : (part + 1) * half],
+            preferred_element_type=jnp.float32,
+        ).astype(jnp.bfloat16)
+
+    def remote(source, target, send, recv, peer):
+        return pltpu.make_async_remote_copy(
+            src_ref=source,
+            dst_ref=target,
+            send_sem=send,
+            recv_sem=recv,
+            device_id=peer,
+            device_id_type=MESH,
+        )
+
+    def z_copy(d):
+        return remote(
+            outgoing_ref.at[flip(z, d), c, carried],
+            member_ref.at[c, z, x, carried],
+            z_send.at[d],
+            z_recv.at[d],
+            at_z(d),
+        )
+
+    def w_copy(d):
+        return remote(
+            weight_ref.at[flip(z, d)], weight_in.at[z], w_send.at[d], w_recv.at[d], at_z(d)
+        )
+
+    def x_copy(d):
+        block = member_ref.at[c, flip(z, d), x, carried]
+        return remote(block, block, x_send.at[d], x_recv.at[d], at_x)
+
+    def y_copy(k):
+        line = x if k % 2 == 0 else 1 - x
+        block = member_ref.at[c, flip(z, k // 2), line, passed]
+        return remote(block, block, y_send.at[k], y_recv.at[k], at_y)
+
+    def c_copy(k):
+        line = x if k % 2 == 0 else 1 - x
+        block = member_ref.at[c, flip(z, k // 2), line]
+        return remote(block, block, c_send.at[k], c_recv.at[k], at_c)
+
+    def p_copy(d):
+        return remote(pair_send.at[d], pair_recv.at[d], p_send.at[d], p_recv.at[d], at_c)
+
+    def f_copy(d):
+        peer = at_x if d in JOIN_FIRST else at_y
+        return remote(first_send.at[d], first_recv.at[d], f_send.at[d], f_recv.at[d], peer)
+
+    def s_copy(d):
+        peer = at_y if d in JOIN_FIRST else at_x
+        return remote(second_send.at[d], second_recv.at[d], s_send.at[d], s_recv.at[d], peer)
+
+    def o_copy(d):
+        return remote(fin_send.at[d], fin_ref.at[z], o_send.at[d], o_recv.at[d], at_z(d))
+
+    started = []
+
+    def start(copy):
+        copy.start()
+        started.append(copy)
+
+    for part in range(2):
+        member_ref[part, z, x] = permuted(z, part)
+    pl.semaphore_wait(barrier, 6)
+    start(x_copy(0))
+    for d in (1, 3, 2):
+        for part in range(2):
+            outgoing_ref[flip(z, d), part] = permuted(flip(z, d), part)
+        start(z_copy(d))
+        start(w_copy(d))
+
+    def compute(d):
+        block = flip(z, d)
+        low = member_ref[0, block].reshape(2 * rows, half)
+        high = member_ref[1, block].reshape(2 * rows, half)
+
+        def project(weights):
+            return jnp.dot(
+                low, weights[:half, :], preferred_element_type=jnp.float32
+            ) + jnp.dot(high, weights[half:, :], preferred_element_type=jnp.float32)
+
+        gate_act = project(gate_ref)
+        up_act = project(up_ref)
+        hidden = (gate_act / (1.0 + jnp.exp(-gate_act)) * up_act).astype(jnp.bfloat16)
+        for yy in range(2):
+            term = jnp.dot(hidden, down_ref[yy * 2 + 1 - c], preferred_element_type=jnp.float32)
+            pair_send[d, yy] = term.astype(jnp.bfloat16).reshape(2, rows, share)
+        start(p_copy(d))
+        for yy in range(2):
+            term = jnp.dot(hidden, down_ref[yy * 2 + c], preferred_element_type=jnp.float32)
+            pair_keep[d, yy] = term.astype(jnp.bfloat16).reshape(2, rows, share)
+
+    def weights_of(d):
+        tile = weight_ref[z] if d == 0 else weight_in[flip(z, d)]
+        mine = jnp.where(x == 0, tile[0:1], tile[1:2])
+        other = jnp.where(x == 0, tile[1:2], tile[0:1])
+
+        def columns(line):
+            square = jnp.transpose(jnp.broadcast_to(line, (rows, rows)))
+            return jnp.concatenate([square] * (share // rows), axis=1)
+
+        return columns(mine), columns(other)
+
+    def wide(value):
+        return value.astype(jnp.float32)
+
+    def stage_first(d):
+        p_copy(d).wait_recv()
+        if d in JOIN_FIRST:
+            for yy in range(2):
+                sums = wide(pair_keep[d, yy, 1 - x]) + wide(pair_recv[d, yy, 1 - x])
+                first_send[d, yy] = sums.astype(jnp.bfloat16)
+            start(f_copy(d))
+            for yy in range(2):
+                first_keep[d, yy] = wide(pair_keep[d, yy, x]) + wide(pair_recv[d, yy, x])
+        else:
+            for line in range(2):
+                sums = wide(pair_keep[d, 1 - y, line]) + wide(pair_recv[d, 1 - y, line])
+                first_send[d, line] = sums.astype(jnp.bfloat16)
+            start(f_copy(d))
+            for line in range(2):
+                first_keep[d, line] = wide(pair_keep[d, y, line]) + wide(pair_recv[d, y, line])
+
+    def stage_second(d):
+        f_copy(d).wait_recv()
+        if d in JOIN_FIRST:
+            if d > 0:
+                w_copy(d).wait_recv()
+            mine, other = weights_of(d)
+            sums = mine * first_keep[d, 1 - y] + other * wide(first_recv[d, 1 - y])
+            second_send[d] = sums.astype(jnp.bfloat16)
+            start(s_copy(d))
+            second_keep[d] = mine * first_keep[d, y] + other * wide(first_recv[d, y])
+        else:
+            sums = first_keep[d, 1 - x] + wide(first_recv[d, 1 - x])
+            second_send[d] = sums.astype(jnp.bfloat16)
+            start(s_copy(d))
+            sums = first_keep[d, x] + wide(first_recv[d, x])
+            second_keep[d] = wide(sums.astype(jnp.bfloat16))
+
+    def stage_last(d):
+        s_copy(d).wait_recv()
+        if d in JOIN_FIRST:
+            result = second_keep[d] + wide(second_recv[d])
+        else:
+            if d > 0:
+                w_copy(d).wait_recv()
+            mine, other = weights_of(d)
+            result = mine * second_keep[d] + other * wide(second_recv[d])
+        if d == 0:
+            fin_ref[z] = result.astype(jnp.bfloat16)
+        else:
+            fin_send[d] = result.astype(jnp.bfloat16)
+            start(o_copy(d))
+
+    def from_z(d):
+        z_copy(d).wait_recv()
+        start(x_copy(d))
+        start(y_copy(2 * d))
+
+    def from_x(d):
+        x_copy(d).wait_recv()
+        start(y_copy(2 * d + 1))
+
+    def from_y(k):
+        y_copy(k).wait_recv()
+        start(c_copy(k))
+
+    from_z(1)
+    from_x(0)
+    for load in loads:
+        load.wait()
+    from_y(2)
+    from_y(1)
+    from_x(1)
+    c_copy(1).wait_recv()
+    compute(0)
+    from_y(3)
+    stage_first(0)
+    c_copy(2).wait_recv()
+    c_copy(3).wait_recv()
+    compute(1)
+    from_z(3)
+    stage_first(1)
+    stage_second(0)
+    from_z(2)
+    from_x(3)
+    from_y(6)
+    from_x(2)
+    from_y(4)
+    from_y(7)
+    stage_second(1)
+    stage_last(0)
+    c_copy(6).wait_recv()
+    c_copy(7).wait_recv()
+    compute(3)
+    from_y(5)
+    stage_first(3)
+    c_copy(4).wait_recv()
+    c_copy(5).wait_recv()
+    compute(2)
+    stage_last(1)
+    stage_first(2)
+    stage_second(3)
+    stage_second(2)
+    stage_last(3)
+    stage_last(2)
+    for d in (1, 3, 2):
+        o_copy(d).wait_recv()
+    for copy in started:
+        copy.wait_send()
+
+
+def expert_exchange(tokens_b, ffn_gain, order, weights, w_gate, w_up, w_down):
+    tok_rows, width = tokens_b.shape
+    rows = tok_rows // GROUPS
+    half = width // 2
+    share = width // 4
+    units = w_gate.shape[2]
+    narrow, full = jnp.bfloat16, jnp.float32
+    vmem = pl.BlockSpec(memory_space=pltpu.VMEM)
+    anywhere = pl.BlockSpec(memory_space=pl.ANY)
+    dma = pltpu.SemaphoreType.DMA
+    return pl.pallas_call(
+        expert_kernel,
+        out_shape=jax.ShapeDtypeStruct((GROUPS, rows, share), narrow),
+        in_specs=[vmem] * 4 + [anywhere] * 3,
+        out_specs=vmem,
+        scratch_shapes=[
+            pltpu.VMEM((tok_rows, width), narrow),
+            pltpu.VMEM((GROUPS, 2, rows, half), narrow),
+            pltpu.VMEM((2, GROUPS, 2, rows, half), narrow),
+            pltpu.VMEM((width, units), narrow),
+            pltpu.VMEM((width, units), narrow),
+            pltpu.VMEM((4, units, share), narrow),
+            pltpu.VMEM(weights.shape, full),
+            pltpu.VMEM((GROUPS, 2, 2, rows, share), narrow),
+            pltpu.VMEM((GROUPS, 2, 2, rows, share), narrow),
+            pltpu.VMEM((GROUPS, 2, 2, rows, share), narrow),
+            pltpu.VMEM((GROUPS, 2, rows, share), narrow),
+            pltpu.VMEM((GROUPS, 2, rows, share), full),
+            pltpu.VMEM((GROUPS, 2, rows, share), narrow),
+            pltpu.VMEM((GROUPS, rows, share), narrow),
+            pltpu.VMEM((GROUPS, rows, share), full),
+            pltpu.VMEM((GROUPS, rows, share), narrow),
+            pltpu.VMEM((GROUPS, rows, share), narrow),
+            dma((6,)),
+        ]
+        + [dma((4,))] * 6
+        + [dma((8,))] * 4
+        + [dma((4,))] * 8,
+        compiler_params=pltpu.CompilerParams(
+            collective_id=0, has_side_effects=True, vmem_limit_bytes=52 * 1024 * 1024
+        ),
+        cost_estimate=pl.CostEstimate(
+            flops=40_000_000_000, bytes_accessed=8_000_000, transcendentals=0
+        ),
+        name="expert_exchange",
+    )(tokens_b, ffn_gain.reshape(1, width), order, weights, w_gate, w_up, w_down)
+
+
+def expert_half_paired(tokens_b, ffn_gain, route_expert, route_weight, w_gate, w_up, w_down):
+    tok_rows = tokens_b.shape[0]
+    group = route_expert[:, 0] // TOPK
+    chosen = (group[:, None] == jnp.arange(GROUPS, dtype=jnp.int32)[None, :]).astype(jnp.bfloat16)
+    line = jnp.arange(tok_rows, dtype=jnp.int32)
+    before = (line[None, :] < line[:, None]).astype(jnp.bfloat16)
+    earlier = jnp.dot(before, chosen, preferred_element_type=jnp.float32)
+    rank = jnp.sum(earlier * chosen.astype(jnp.float32), axis=1).astype(jnp.int32)
+    place = group * (tok_rows // GROUPS) + rank
+    hit = line[:, None] == place[None, :]
+    order = hit.astype(jnp.bfloat16)
+    first_even = route_expert[:, 0] % TOPK == 0
+    even = jnp.where(first_even, route_weight[:, 0], route_weight[:, 1])
+    odd = jnp.where(first_even, route_weight[:, 1], route_weight[:, 0])
+    sorted_even = jnp.sum(jnp.where(hit, even[None, :], 0.0), axis=1)
+    sorted_odd = jnp.sum(jnp.where(hit, odd[None, :], 0.0), axis=1)
+    rows = tok_rows // GROUPS
+    weights = jnp.stack([sorted_even.reshape(GROUPS, rows), sorted_odd.reshape(GROUPS, rows)], axis=1)
+    weights = jnp.pad(weights, ((0, 0), (0, 8 - TOPK), (0, 0)))
+    fin = expert_exchange(tokens_b, ffn_gain, order, weights, w_gate, w_up, w_down)
+    fin = fin.reshape(tok_rows, fin.shape[2])
+    back = lax.dot_general(order, fin, (((0,), (0,)), ((), ())), preferred_element_type=jnp.float32)
+    return back.astype(jnp.bfloat16)
 
 
 def body(
@@ -225,7 +623,14 @@
         w_value,
         w_out,
     )
-    moe_out = expert_half(tokens_b, ffn_gain, route_expert, route_weight, w_gate, w_up, w_down)
+    paired = (
+        lax.axis_size("ep") == GROUPS * TOPK
+        and lax.axis_size("tp") == 4
+        and GROUPS == 4
+        and tokens_b.shape[0] == GROUPS * 128
+    )
+    experts = expert_half_paired if paired else expert_half
+    moe_out = experts(tokens_b, ffn_gain, route_expert, route_weight, w_gate, w_up, w_down)
     return (mixer_out, moe_out)
 
 

time: 207 us -> 128 us (0.62)
  Pallas kernels: 0 us -> 72.6 us
  blocking collectives: 90.5 us -> 30.2 us
  waiting for transfers between devices: 45.7 us -> 0.02 us
  local copies, waits for them, and re-layouts: 18.2 us -> 2.65 us
  other arithmetic: 15.2 us -> 2.25 us
  matrix products: 18.1 us -> 6.05 us
  starting transfers between devices: 4.65 us -> 0.04 us
    pallas_call x0 -> x1, Pallas kernels: none -> 72.6 us  [expert_exchange(): pl.pallas_call(expert_kernel, out_shape=jax.ShapeDtypeStruct((GROUPS, row...]
    all_gather x1 -> x0, waiting for transfers between devices: 33.6 us -> none  [expert_half(): member = lax.all_gather(arrived, 'tp', axis=1, tiled=True)]
    all_to_all x1 -> x0, blocking collectives: 32.9 us -> none  [expert_half(): lax.all_to_all(own_cols, 'ep', split_axis=0, concat_axis=0, tiled=True)]
    all_gather x2 -> x1, blocking collectives: 57.6 us -> 30.2 us  [mixer_half(): lax.all_gather(jnp.concatenate([key_latent, key_rot], axis=1), 'ep', axis...]
    all_to_all x1 -> x0, waiting for transfers between devices: 12 us -> none  [expert_half(): lax.all_to_all(shared, 'ep', split_axis=0, concat_axis=0, tiled=True)]
    dot_general x2, matrix products: 13.3 us -> 1.55 us  [the longest x1 1.29 us: expert_half_paired(): lax.dot_general(order, fin, (((0,), (0,)), ((), ())), preferred_element_t...]
    gather x3 -> x0, local copies, waits for them, and re-layouts: 10.4 us -> none  [the longest x1 6.02 us: expert_half(): outgoing = jnp.take(normed, source_row, axis=0)]
    reduce_sum x2 -> x1, other arithmetic: 5.23 us -> 0.36 us  [expert_half_paired(): sorted_even = jnp.sum(jnp.where(hit, even[None, :], 0.0), axis=1)]
  transfers between devices with their start and end apart: 4 -> 1, of which waited for: 2 -> 0; matrix products, arithmetic and copies ran while one was open for 8% -> 2% of each run, Pallas kernels for 0% -> 57%
where the time goes in v1:
time: 128 us
  Pallas kernels  72.6 us (57%)
  blocking collectives  30.2 us (24%)
  between operations  14.4 us (11%)
  matrix products  6.05 us (5%)
  local copies, waits for them, and re-layouts  2.65 us (2%)
  other arithmetic  2.25 us (2%)
    pallas_call x1, Pallas kernels, expert_exchange(): pl.pallas_call(expert_kernel, out_shape=jax.ShapeDtypeStruct((GROUPS, row...  72.6 us
    all_gather x1, blocking collectives, mixer_half(): lax.all_gather(jnp.concatenate([key_latent, key_rot], axis=1), 'ep', axis...  30.2 us
  transfers between devices with their start and end apart: 1, of which 0 were waited for; matrix products, arithmetic and copies ran while one was open for 2% of the time, Pallas kernels for 57%

profile of v1, /device:TPU:0, one launch (start us, length us, event | category | flops | bytes accessed | tf_op | source)
XLA Modules:
  0.0 128.2 jit_solution(13821611436855454483)
XLA Ops:
  7.2 0.0 copy-start
  7.2 0.0 copy-start.2
  7.2 0.0 copy-start.4
  7.2 0.0 copy-start.3
  7.2 0.0 copy-start.9
  7.2 0.0 copy-start.7
  7.2 0.0 reduce-scatter.2.cloned.1.call-start
  7.3 0.8 slice.30
  8.1 0.7 slice.31
  8.9 1.0 fusion.16
  9.9 1.3 fusion.24
  11.2 0.1 broadcast_multiply_fusion.1
  11.3 0.1 fusion.31
  11.5 1.0 copy.20
  12.5 30.2 %all_gather.3 = bf16[1024,320]{0,1:T(8,128)(2,1)S(1)} all-gather(bf16[128,320]{0,1:T(8,128)(2,1)S(1)} %pad_maximum_fusion), channel_id=1, replica_groups=mesh['ep'=8,'tp'=4] {'ep'}, dimensions={0}, use_global_device_ids=true | all-gather | bytes 737280 | tf_op jit(solution)/shard_map/all_gather | solution.py:143
  42.6 0.1 fusion.7
  42.8 0.0 copy-done.2
  42.8 0.0 copy-done.4
  42.8 0.0 copy-done.3
  42.8 0.2 fusion.5
  43.0 0.0 copy-done.9
  43.0 0.0 copy-done.7
  43.0 0.4 convolution_convert_fusion.3
  43.4 0.0 copy-start.8
  43.5 0.3 fusion.21
  43.7 0.4 fusion.45
  44.2 0.3 fusion.11
  44.5 0.0 copy-done.8
  44.5 0.4 convolution_convert_fusion.2
  44.9 0.0 copy-start.6
  44.9 0.0 copy-start.5
  44.9 0.0 copy-start.1
  44.9 0.4 fusion.4
  45.3 0.0 copy-done
  45.4 1.1 convolution_convert_fusion
  46.5 0.0 reduce-scatter.2.cloned.1.call-update
  46.5 0.0 copy-done.6
  46.5 0.0 copy-done.5
  46.6 0.3 fusion.6
  46.8 0.1 fusion.10.order_ref
  47.0 0.4 select_reduce_fusion.1
  47.4 0.0 copy-done.1
  47.4 72.6 %expert_exchange.1 = bf16[4,128,512]{2,1,0:T(8,128)(2,1)S(1)} custom-call(bf16[512,2048]{1,0:T(8,128)(2,1)} %tokens_ref.1, f32[1,2048]{1,0:T(1,128)S(1)} %bitcast.62, bf16[512,512]{1,0:T(8,128)(2,1)S(1)} %fusion.10.order_ref, f32[4,8,128]{2,1,0:T(8,128)S(1)} %select_maximum_fusion.weight_ref, bf16[1,2048,256]{2,1,0:T(8,128)(2,1)} %gate_hbm.1, ...), custom_call_target="tpu_custom_call" | custom-call | flops 40000000000 | bytes 8000000 | tf_op jit(solution)/shard_map/expert_exchange/pallas_call | solution.py:532
  120.0 1.3 %convolution_convert_fusion.1 = bf16[512,512]{1,0:T(8,128)(2,1)} fusion(bf16[512,512]{1,0:T(8,128)(2,1)S(1)} %bitcast.63, s32[512]{0:T(512)S(1)} %fusion.36), kind=kOutput, calls=%fused_computation.6 | convolution fusion | flops 268959744 | bytes 1050624 | tf_op jit(solution)/shard_map/dot_general | solution.py:591
  121.3 0.0 reduce-scatter.2.cloned.1.call-done
  (19 shorter events, 0.2 us)
Async XLA Ops:
  7.2 38.2 %copy-start = (bf16[256,2048]{1,0:T(8,128)(2,1)S(1)}, bf16[256,2048]{1,0:T(8,128)(2,1)}, u32[]{:S(2)}) copy-start(bf16[256,2048]{1,0:T(8,128)(2,1)} %param.26) | copy-start | bytes 3145732
  7.2 35.6 %copy-start.2 = (bf16[128,512]{1,0:T(8,128)(2,1)S(1)}, bf16[128,512]{1,0:T(8,128)(2,1)}, u32[]{:S(2)}) copy-start(bf16[128,512]{1,0:T(8,128)(2,1)} %param.17) | copy-start | bytes 393220
  7.2 35.6 %copy-start.4 = (f32[512]{0:T(512)S(1)}, f32[512]{0:T(512)}, u32[]{:S(2)}) copy-start(f32[512]{0:T(512)} %param.20) | copy-start | bytes 6148
  7.2 35.6 %copy-start.3 = (bf16[512,256]{1,0:T(8,128)(2,1)S(1)}, bf16[512,256]{1,0:T(8,128)(2,1)}, u32[]{:S(2)}) copy-start(bf16[512,256]{1,0:T(8,128)(2,1)} %param.22) | copy-start | bytes 786436
  7.2 35.8 %copy-start.9 = (f32[256]{0:T(256)S(1)}, f32[256]{0:T(256)}, u32[]{:S(2)}) copy-start(f32[256]{0:T(256)} %param.21) | copy-start | bytes 3076
  7.2 35.8 %copy-start.7 = (bf16[256,256]{1,0:T(8,128)(2,1)S(1)}, bf16[256,256]{1,0:T(8,128)(2,1)}, u32[]{:S(2)}) copy-start(bf16[256,256]{1,0:T(8,128)(2,1)} %param.24) | copy-start | bytes 393220
  7.2 114.1 %reduce-scatter.2.cloned.1.call-start = ((), (), s32[]{:S(2)}) async-start(), calls=%async_computation.1 | async-start | bytes 655360 | tf_op jit(solution)/shard_map/reduce_scatter | solution.py:151
  43.4 1.1 copy-start.8
  44.9 1.6 %copy-start.6 = (s32[512,2]{0,1:T(2,128)S(1)}, s32[512,2]{0,1:T(2,128)}, u32[]{:S(2)}) copy-start(s32[512,2]{0,1:T(2,128)} %param.29) | copy-start | bytes 12292
  44.9 1.6 %copy-start.5 = (f32[512,2]{0,1:T(2,128)S(1)}, f32[512,2]{0,1:T(2,128)}, u32[]{:S(2)}) copy-start(f32[512,2]{0,1:T(2,128)} %param.30) | copy-start | bytes 12292
  44.9 2.4 %copy-start.1 = (f32[2048]{0:T(1024)S(1)}, f32[2048]{0:T(1024)}, u32[]{:S(2)}) copy-start(f32[2048]{0:T(1024)} %param.28) | copy-start | bytes 24580
Sparse Core Ops, SparseCore 0:
  46.6 20.8 reduce-scatter.1

commit v2 on v1

--- a/solution.py
+++ b/solution.py
@@ -14,8 +14,8 @@
 TOPK = 2
 GROUPS = 4
 MESH = pl.DeviceIdType.MESH
-SPLIT_NUM, SPLIT_DEN = 3, 8
-JOIN_FIRST = (1, 3)
+SPLIT_NUM, SPLIT_DEN = 1, 8
+JOIN_FIRST = ()
 
 
 epsilon = 1e-06
@@ -215,7 +215,20 @@
     gate_hbm,
     up_hbm,
     down_hbm,
+    query_ref,
+    latent_ref,
+    rope_ref,
+    query_gain_ref,
+    key_gain_ref,
+    cosine_ref,
+    sine_ref,
+    w_query_ref,
+    w_rope_ref,
+    w_key_ref,
+    w_value_ref,
+    w_out_ref,
     fin_ref,
+    mixer_ref,
     normed_ref,
     outgoing_ref,
     member_ref,
@@ -233,6 +246,12 @@
     second_keep,
     second_recv,
     fin_send,
+    keys_ref,
+    heads_ref,
+    mixed_ref,
+    mixed_in,
+    joint_send,
+    joint_recv,
     load_sem,
     z_send,
     z_recv,
@@ -252,6 +271,16 @@
     s_recv,
     o_send,
     o_recv,
+    kz_send,
+    kz_recv,
+    kx_send,
+    kx_recv,
+    kc_send,
+    kc_recv,
+    a_send,
+    a_recv,
+    j_send,
+    j_recv,
 ):
     ep = lax.axis_index("ep")
     tp = lax.axis_index("tp")
@@ -289,17 +318,35 @@
     for load in loads:
         load.start()
 
+    def scaled(values_in, gain):
+        widened = values_in.astype(jnp.float32)
+        mean = jnp.mean(widened * widened, axis=-1, keepdims=True)
+        return (widened * lax.rsqrt(mean + epsilon) * gain).astype(jnp.bfloat16)
+
+    turn_shape = (w_rope_ref.shape[1], w_rope_ref.shape[1])
+    from_lane = lax.broadcasted_iota(jnp.int32, turn_shape, 0)
+    to_lane = lax.broadcasted_iota(jnp.int32, turn_shape, 1)
+    to_even = to_lane % 2 == 0
+    swap = jnp.where(to_even & (from_lane == to_lane + 1), -1.0, 0.0)
+    swap = jnp.where(jnp.logical_not(to_even) & (from_lane == to_lane - 1), 1.0, swap)
+    swap = swap.astype(jnp.bfloat16)
+
+    def dot(left, right):
+        return jnp.dot(left, right, preferred_element_type=jnp.float32)
+
+    attend_rows, rank = latent_ref.shape
+    rope_twice = jnp.concatenate([rope_ref[...]] * 2, axis=1)
+    key_turn = rope_twice.astype(jnp.float32) * cosine_ref[...]
+    key_turn = key_turn + dot(rope_twice, swap) * sine_ref[...]
+    keys_ref[z, x, :, :rank] = scaled(latent_ref[...], key_gain_ref[...])
+    keys_ref[z, x, :, rank:] = key_turn.astype(jnp.bfloat16)
+
     step_rows = 32
 
     def norm_step(step, unused):
         lines = pl.ds(pl.multiple_of(step * step_rows, step_rows), step_rows)
-        widened = tokens_ref[lines, :].astype(jnp.float32)
-        mean = jnp.mean(widened * widened, axis=-1, keepdims=True)
-        normed = widened * lax.rsqrt(mean + epsilon) * gain_ref[...]
-        normed_ref[lines, :] = normed.astype(jnp.bfloat16)
+        normed_ref[lines, :] = scaled(tokens_ref[lines, :], gain_ref[...])
         return unused
-
-    lax.fori_loop(0, tok_rows // step_rows, norm_step, 0)
 
     def permuted(group, part):
         lines = pl.ds(pl.multiple_of(group * rows, rows), rows)
@@ -361,15 +408,44 @@
     def o_copy(d):
         return remote(fin_send.at[d], fin_ref.at[z], o_send.at[d], o_recv.at[d], at_z(d))
 
+    key_half = pl.ds(pl.multiple_of(c * (attend_rows // 2), 16), attend_rows // 2)
+
+    def kz_copy(d):
+        block = keys_ref.at[z, x, key_half]
+        return remote(block, block, kz_send.at[d], kz_recv.at[d], at_z(d))
+
+    def kx_copy(d):
+        block = keys_ref.at[flip(z, d), x, key_half]
+        return remote(block, block, kx_send.at[d], kx_recv.at[d], at_x)
+
+    def kc_copy(d):
+        if d == 0:
+            block = keys_ref.at[z, 1 - x, key_half]
+        else:
+            block = keys_ref.at[flip(z, d), :, key_half]
+        return remote(block, block, kc_send.at[d], kc_recv.at[d], at_c)
+
+    def a_copy(yy):
+        return remote(
+            mixed_ref.at[yy * 2 + 1 - c], mixed_in.at[yy], a_send.at[yy], a_recv.at[yy], at_c
+        )
+
+    def j_copy():
+        return remote(joint_send, joint_recv, j_send.at[0], j_recv.at[0], at_y)
+
     started = []
 
     def start(copy):
         copy.start()
         started.append(copy)
 
+    pl.semaphore_wait(barrier, 6)
+    start(kx_copy(0))
+    for d in (1, 3, 2):
+        start(kz_copy(d))
+    lax.fori_loop(0, tok_rows // step_rows, norm_step, 0)
     for part in range(2):
         member_ref[part, z, x] = permuted(z, part)
-    pl.semaphore_wait(barrier, 6)
     start(x_copy(0))
     for d in (1, 3, 2):
         for part in range(2):
@@ -408,6 +484,51 @@
             return jnp.concatenate([square] * (share // rows), axis=1)
 
         return columns(mine), columns(other)
+
+    def attend():
+        query_normed = scaled(query_ref[...], query_gain_ref[...])
+        query_nope = dot(query_normed, w_query_ref[...]).astype(jnp.bfloat16)
+        swapped = dot(w_rope_ref[...], swap).astype(jnp.bfloat16)
+        query_turn = dot(query_normed, w_rope_ref[...]) * cosine_ref[...]
+        query_turn = query_turn + dot(query_normed, swapped) * sine_ref[...]
+        query_turn = query_turn.astype(jnp.bfloat16)
+        count = keys_ref.shape[0] * keys_ref.shape[1] * attend_rows
+        keys = keys_ref[...].reshape(count, keys_ref.shape[3])
+        latents, turned = keys[:, :rank], keys[:, rank:]
+        key_nope = dot(latents, w_key_ref[...]).astype(jnp.bfloat16)
+        value_rows = dot(latents, w_value_ref[...]).astype(jnp.bfloat16)
+        lane = lax.broadcasted_iota(jnp.int32, query_turn.shape, 1)
+        for head in range(w_query_ref.shape[1] // NOPE):
+            own = slice(head * NOPE, (head + 1) * NOPE)
+            part = jnp.where(lane // ROPE == head, query_turn, jnp.zeros_like(query_turn))
+            scores = lax.dot_general(
+                jnp.concatenate([query_nope[:, own], part], axis=1),
+                jnp.concatenate([key_nope[:, own], turned], axis=1),
+                (((1,), (1,)), ((), ())),
+                preferred_element_type=jnp.float32,
+            )
+            scores = scores * (NOPE + ROPE) ** (-0.5)
+            raised = jnp.exp(scores - jnp.max(scores, axis=-1, keepdims=True))
+            totals = jnp.sum(raised, axis=-1, keepdims=True)
+            mixed = dot(raised.astype(jnp.bfloat16), value_rows[:, own]) / totals
+            heads_ref[:, own] = mixed.astype(jnp.bfloat16)
+        for t in range(4):
+            lines = slice(t * (attend_rows // 4), (t + 1) * (attend_rows // 4))
+            mixed_ref[t] = dot(heads_ref[lines, :], w_out_ref[...]).astype(jnp.bfloat16)
+        for yy in range(2):
+            start(a_copy(yy))
+
+    def attend_join():
+        for yy in range(2):
+            a_copy(yy).wait_recv()
+        sums = wide(mixed_ref[(1 - y) * 2 + c]) + wide(mixed_in[1 - y])
+        joint_send[...] = sums.astype(jnp.bfloat16)
+        start(j_copy())
+
+    def attend_last():
+        j_copy().wait_recv()
+        sums = wide(mixed_ref[y * 2 + c]) + wide(mixed_in[y]) + wide(joint_recv[...])
+        mixer_ref[...] = sums.astype(jnp.bfloat16)
 
     def wide(value):
         return value.astype(jnp.float32)
@@ -474,6 +595,12 @@
         y_copy(k).wait_recv()
         start(c_copy(k))
 
+    for d in (1, 3, 2):
+        kz_copy(d).wait_recv()
+        start(kx_copy(d))
+    for d in (0, 1, 3, 2):
+        kx_copy(d).wait_recv()
+        start(kc_copy(d))
     from_z(1)
     from_x(0)
     for load in loads:
@@ -487,8 +614,11 @@
     stage_first(0)
     c_copy(2).wait_recv()
     c_copy(3).wait_recv()
+    from_z(3)
     compute(1)
-    from_z(3)
+    for d in range(4):
+        kc_copy(d).wait_recv()
+    attend()
     stage_first(1)
     stage_second(0)
     from_z(2)
@@ -504,12 +634,14 @@
     compute(3)
     from_y(5)
     stage_first(3)
+    attend_join()
     c_copy(4).wait_recv()
     c_copy(5).wait_recv()
     compute(2)
     stage_last(1)
     stage_first(2)
     stage_second(3)
+    attend_last()
     stage_second(2)
     stage_last(3)
     stage_last(2)
@@ -519,21 +651,27 @@
         copy.wait_send()
 
 
-def expert_exchange(tokens_b, ffn_gain, order, weights, w_gate, w_up, w_down):
+def expert_exchange(tokens_b, ffn_gain, order, weights, w_gate, w_up, w_down, mixer_args):
     tok_rows, width = tokens_b.shape
     rows = tok_rows // GROUPS
     half = width // 2
     share = width // 4
     units = w_gate.shape[2]
+    attend_rows, rank = mixer_args[1].shape
+    key_cols = rank + 2 * ROPE
+    head_cols = mixer_args[7].shape[1]
     narrow, full = jnp.bfloat16, jnp.float32
     vmem = pl.BlockSpec(memory_space=pltpu.VMEM)
     anywhere = pl.BlockSpec(memory_space=pl.ANY)
     dma = pltpu.SemaphoreType.DMA
     return pl.pallas_call(
         expert_kernel,
-        out_shape=jax.ShapeDtypeStruct((GROUPS, rows, share), narrow),
-        in_specs=[vmem] * 4 + [anywhere] * 3,
-        out_specs=vmem,
+        out_shape=(
+            jax.ShapeDtypeStruct((GROUPS, rows, share), narrow),
+            jax.ShapeDtypeStruct((attend_rows // 4, width), narrow),
+        ),
+        in_specs=[vmem] * 4 + [anywhere] * 3 + [vmem] * 12,
+        out_specs=(vmem, vmem),
         scratch_shapes=[
             pltpu.VMEM((tok_rows, width), narrow),
             pltpu.VMEM((GROUPS, 2, rows, half), narrow),
@@ -552,11 +690,18 @@
             pltpu.VMEM((GROUPS, rows, share), full),
             pltpu.VMEM((GROUPS, rows, share), narrow),
             pltpu.VMEM((GROUPS, rows, share), narrow),
+            pltpu.VMEM((GROUPS, 2, attend_rows, key_cols), narrow),
+            pltpu.VMEM((attend_rows, head_cols), narrow),
+            pltpu.VMEM((4, attend_rows // 4, width), narrow),
+            pltpu.VMEM((2, attend_rows // 4, width), narrow),
+            pltpu.VMEM((attend_rows // 4, width), narrow),
+            pltpu.VMEM((attend_rows // 4, width), narrow),
             dma((6,)),
         ]
         + [dma((4,))] * 6
         + [dma((8,))] * 4
-        + [dma((4,))] * 8,
+        + [dma((4,))] * 14
+        + [dma((2,))] * 4,
         compiler_params=pltpu.CompilerParams(
             collective_id=0, has_side_effects=True, vmem_limit_bytes=52 * 1024 * 1024
         ),
@@ -564,10 +709,24 @@
             flops=40_000_000_000, bytes_accessed=8_000_000, transcendentals=0
         ),
         name="expert_exchange",
-    )(tokens_b, ffn_gain.reshape(1, width), order, weights, w_gate, w_up, w_down)
-
-
-def expert_half_paired(tokens_b, ffn_gain, route_expert, route_weight, w_gate, w_up, w_down):
+    )(tokens_b, ffn_gain.reshape(1, width), order, weights, w_gate, w_up, w_down, *mixer_args)
+
+
+def lane_tables(tok_rows, width):
+    positions = lax.axis_index("ep") * tok_rows + lax.broadcasted_iota(
+        jnp.int32, (tok_rows, width), 0
+    )
+    pair = lax.broadcasted_iota(jnp.int32, (tok_rows, width), 1) % ROPE // 2
+    half_width = ROPE // 2
+    quarter = half_width // 2
+    inverse = rotary_base ** (-(pair % quarter * 2).astype(jnp.float32) / half_width)
+    grid_row = (positions // GRID_W).astype(jnp.float32)
+    grid_col = (positions % GRID_W).astype(jnp.float32)
+    angle = jnp.where(pair < quarter, grid_row, grid_col) * inverse
+    return (jnp.cos(angle), jnp.sin(angle))
+
+
+def paired(mixer, tokens_b, ffn_gain, route_expert, route_weight, w_gate, w_up, w_down):
     tok_rows = tokens_b.shape[0]
     group = route_expert[:, 0] // TOPK
     chosen = (group[:, None] == jnp.arange(GROUPS, dtype=jnp.int32)[None, :]).astype(jnp.bfloat16)
@@ -586,10 +745,22 @@
     rows = tok_rows // GROUPS
     weights = jnp.stack([sorted_even.reshape(GROUPS, rows), sorted_odd.reshape(GROUPS, rows)], axis=1)
     weights = jnp.pad(weights, ((0, 0), (0, 8 - TOPK), (0, 0)))
-    fin = expert_exchange(tokens_b, ffn_gain, order, weights, w_gate, w_up, w_down)
+    query_latent, key_latent, rope_key, query_gain, key_gain = mixer[:5]
+    mixer_args = (
+        query_latent,
+        key_latent,
+        rope_key,
+        query_gain.reshape(1, -1),
+        key_gain.reshape(1, -1),
+        *lane_tables(query_latent.shape[0], 2 * ROPE),
+        *mixer[5:],
+    )
+    fin, mixer_out = expert_exchange(
+        tokens_b, ffn_gain, order, weights, w_gate, w_up, w_down, mixer_args
+    )
     fin = fin.reshape(tok_rows, fin.shape[2])
     back = lax.dot_general(order, fin, (((0,), (0,)), ((), ())), preferred_element_type=jnp.float32)
-    return back.astype(jnp.bfloat16)
+    return (mixer_out, back.astype(jnp.bfloat16))
 
 
 def body(
@@ -611,7 +782,7 @@
     w_up,
     w_down,
 ):
-    mixer_out = mixer_half(
+    mixer = (
         query_latent,
         key_latent,
         rope_key,
@@ -623,15 +794,16 @@
         w_value,
         w_out,
     )
-    paired = (
+    experts = (tokens_b, ffn_gain, route_expert, route_weight, w_gate, w_up, w_down)
+    if (
         lax.axis_size("ep") == GROUPS * TOPK
         and lax.axis_size("tp") == 4
         and GROUPS == 4
         and tokens_b.shape[0] == GROUPS * 128
-    )
-    experts = expert_half_paired if paired else expert_half
-    moe_out = experts(tokens_b, ffn_gain, route_expert, route_weight, w_gate, w_up, w_down)
-    return (mixer_out, moe_out)
+        and w_query.shape[1] == 2 * NOPE
+    ):
+        return paired(mixer, *experts)
+    return (mixer_half(*mixer), expert_half(*experts))
 
 
 def solution(mesh):

time: 128 us -> 90.7 us (0.71)
  blocking collectives: 30.2 us -> 0 us
  between operations: 14.4 us -> 0.71 us
  local copies, waits for them, and re-layouts: 2.65 us -> 9.71 us
  matrix products: 6.05 us -> 1.55 us
  Pallas kernels: 72.6 us -> 75.8 us
    all_gather x1 -> x0, blocking collectives: 30.2 us -> none  [mixer_half(): lax.all_gather(jnp.concatenate([key_latent, key_rot], axis=1), 'ep', axis...]
    unnamed x21 -> x20, local copies, waits for them, and re-layouts: 1.01 us -> 8.94 us
    dot_general x10 -> x2, matrix products: 6.05 us -> 1.55 us  [the longest x1 1.29 us: paired(): lax.dot_general(order, fin, (((0,), (0,)), ((), ())), preferred_element_t...]
    pallas_call x1, Pallas kernels: 72.6 us -> 75.8 us  [expert_exchange(): pl.pallas_call(expert_kernel, out_shape=(jax.ShapeDtypeStruct((GROUPS, ro...]
    reduce_sum x4 -> x1, other arithmetic: 1.8 us -> 0.36 us  [paired(): sorted_even = jnp.sum(jnp.where(hit, even[None, :], 0.0), axis=1)]
  transfers between devices with their start and end apart: 1 -> 0, of which waited for: 0 -> 0; matrix products, arithmetic and copies ran while one was open for 2% -> 0% of each run, Pallas kernels for 57% -> 0%
where the time goes in v2:
time: 90.7 us; the launch traced here: 90.2 us
  Pallas kernels  75.8 us (84%)
  local copies, waits for them, and re-layouts  9.71 us (11%)
  other arithmetic  2.43 us (3%)
  matrix products  1.55 us (2%)
    pallas_call x1, Pallas kernels, expert_exchange(): pl.pallas_call(expert_kernel, out_shape=(jax.ShapeDtypeStruct((GROUPS, ro...  75.8 us
    unnamed x20, local copies, waits for them, and re-layouts  8.94 us

profile of v2, /device:TPU:0, one launch (start us, length us, event | category | flops | bytes accessed | tf_op | source)
XLA Modules:
  0.0 90.2 jit_solution(13565013184280229441)
XLA Ops:
  0.7 0.7 fusion.26
  1.4 0.3 fusion
  1.7 0.8 fusion.25
  2.5 0.4 select_reduce_fusion.1
  2.8 0.8 copy.19.rope_ref
  3.7 0.4 fusion.15
  4.0 0.9 %fusion.1.order_ref = bf16[512,512]{1,0:T(8,128)(2,1)} fusion(s32[512]{0:T(512)S(1)} %fusion.20), kind=kLoop, calls=%fused_computation.7 | loop fusion | flops 524288 | bytes 526336 | tf_op jit(solution)/shard_map/convert_element_type | solution.py:739
  5.0 0.0 copy-start
  5.0 0.9 %copy-done = bf16[512,256]{1,0:T(8,128)(2,1)S(1)} copy-done((bf16[512,256]{1,0:T(8,128)(2,1)S(1)}, bf16[512,256]{1,0:T(8,128)(2,1)}, u32[]{:S(2)}) %copy-start) | copy-done | bytes 262168
  5.9 0.0 copy-start.1
  5.9 0.9 %copy-done.1 = bf16[128,512]{1,0:T(8,128)(2,1)S(1)} copy-done((bf16[128,512]{1,0:T(8,128)(2,1)S(1)}, bf16[128,512]{1,0:T(8,128)(2,1)}, u32[]{:S(2)}) %copy-start.1) | copy-done | bytes 131096
  6.8 0.0 copy-start.2
  6.8 0.9 %copy-done.2 = bf16[512,128]{1,0:T(8,128)(2,1)S(1)} copy-done((bf16[512,128]{1,0:T(8,128)(2,1)S(1)}, bf16[512,128]{1,0:T(8,128)(2,1)}, u32[]{:S(2)}) %copy-start.2) | copy-done | bytes 131096
  7.7 0.0 copy-start.3
  7.7 0.9 %copy-done.3 = bf16[256,256]{1,0:T(8,128)(2,1)S(1)} copy-done((bf16[256,256]{1,0:T(8,128)(2,1)S(1)}, bf16[256,256]{1,0:T(8,128)(2,1)}, u32[]{:S(2)}) %copy-start.3) | copy-done | bytes 131096
  8.6 0.0 copy-start.4
  8.6 0.9 %copy-done.4 = bf16[256,256]{1,0:T(8,128)(2,1)S(1)} copy-done((bf16[256,256]{1,0:T(8,128)(2,1)S(1)}, bf16[256,256]{1,0:T(8,128)(2,1)}, u32[]{:S(2)}) %copy-start.4) | copy-done | bytes 131096
  9.5 0.0 copy-start.5
  9.5 0.8 copy-done.5
  10.4 0.0 copy-start.6
  10.4 0.7 copy-done.6
  11.1 0.0 copy-start.7
  11.1 0.7 copy-done.7
  11.8 0.0 copy-start.8
  11.8 0.7 copy-done.8
  12.4 75.8 %expert_exchange.1 = (bf16[4,128,512]{2,1,0:T(8,128)(2,1)S(1)}, bf16[32,2048]{1,0:T(8,128)(2,1)S(1)}) custom-call(bf16[512,2048]{1,0:T(8,128)(2,1)} %tokens_ref.1, f32[1,2048]{1,0:T(1,128)S(1)} %bitcast.11, bf16[512,512]{1,0:T(8,128)(2,1)} %fusion.1.order_ref, f32[4,8,128]{2,1,0:T(8,128)S(1)} %select_maximum_fusion.weight_ref, ...), custom_call_target="tpu_custom_call" | custom-call | flops 40000000000 | bytes 8000000 | tf_op jit(solution)/shard_map/expert_exchange/pallas_call | solution.py:667
  88.3 1.3 %convolution_convert_fusion = bf16[512,512]{1,0:T(8,128)(2,1)} fusion(bf16[512,512]{1,0:T(8,128)(2,1)S(1)} %bitcast.14, s32[512]{0:T(512)S(1)} %fusion.20), kind=kOutput, calls=%fused_computation | convolution fusion | flops 268959744 | bytes 1050624 | tf_op jit(solution)/shard_map/dot_general | solution.py:762
  89.5 0.7 copy.21
  (8 shorter events, 0.1 us)
Async XLA Ops:
  5.0 0.9 %copy-start = (bf16[512,256]{1,0:T(8,128)(2,1)S(1)}, bf16[512,256]{1,0:T(8,128)(2,1)}, u32[]{:S(2)}) copy-start(bf16[512,256]{1,0:T(8,128)(2,1)} %w_query_ref.1) | copy-start | bytes 786436
  5.9 0.9 %copy-start.1 = (bf16[128,512]{1,0:T(8,128)(2,1)S(1)}, bf16[128,512]{1,0:T(8,128)(2,1)}, u32[]{:S(2)}) copy-start(bf16[128,512]{1,0:T(8,128)(2,1)} %query_ref.1) | copy-start | bytes 393220
  6.8 0.9 %copy-start.2 = (bf16[512,128]{1,0:T(8,128)(2,1)S(1)}, bf16[512,128]{1,0:T(8,128)(2,1)}, u32[]{:S(2)}) copy-start(bf16[512,128]{1,0:T(8,128)(2,1)} %w_rope_ref.1) | copy-start | bytes 393220
  7.7 0.9 %copy-start.3 = (bf16[256,256]{1,0:T(8,128)(2,1)S(1)}, bf16[256,256]{1,0:T(8,128)(2,1)}, u32[]{:S(2)}) copy-start(bf16[256,256]{1,0:T(8,128)(2,1)} %w_key_ref.1) | copy-start | bytes 393220
  8.6 0.9 %copy-start.4 = (bf16[256,256]{1,0:T(8,128)(2,1)S(1)}, bf16[256,256]{1,0:T(8,128)(2,1)}, u32[]{:S(2)}) copy-start(bf16[256,256]{1,0:T(8,128)(2,1)} %w_value_ref.1) | copy-start | bytes 393220
  9.5 0.8 copy-start.5
  10.4 0.7 copy-start.6
  11.1 0.7 copy-start.7
  11.8 0.7 copy-start.8
